TPU v7x, 32 devices: a whole 2x2x4 slice. The times are simulated.
32 devices in a mesh: ep: 8 (over z, x), tp: 4 (over y, core).
Axes of the slice: x: 2, y: 2, z: 4, core: 2. Of those that a mesh axis runs over, the one named last changes fastest.
Arguments:
- queries: bfloat16 [1024, 1024], P('ep', 'tp'), may hold values from -6 to 6
- key_states: bfloat16 [1024, 256], P('ep'), may hold values from -192 to 192
- value_states: bfloat16 [1024, 256], P('ep'), may hold values from -12 to 12
- sink_logit: float32 [16], P('tp'), may hold values from 3 to 7
- out_weight: bfloat16 [1024, 2048], P('tp'), may hold values from -0.1875 to 0.1875
- expert_input: bfloat16 [1024, 2048], P('ep'), may hold values from -6 to 6
- norm_gain: float32 [2048], replicated, may hold values from 0.1 to 1.9
- routes: int32 [1024, 2], P('ep'), may hold values from 0 to 7, all different within a row; in each aligned block of 128 rows (0 to 127, 128 to 255, ...) at most 40 rows name the same one
- route_weight: float32 [1024, 2], P('ep'), may hold values from 0.1 to 1
- gate_weight: bfloat16 [8, 2048, 4096], P('ep', None, 'tp'), may hold values from -0.125 to 0.125
- up_weight: bfloat16 [8, 2048, 4096], P('ep', None, 'tp'), may hold values from -0.125 to 0.125
- down_weight: bfloat16 [8, 4096, 2048], P('ep', 'tp'), may hold values from -0.125 to 0.125
Outputs:
- mixer_out: bfloat16 [1024, 2048], P(('ep', 'tp'))
- expert_out: bfloat16 [1024, 2048], P('ep', 'tp')
Inputs may be any that keep to these rules, and one draw needn't show every extreme that they name: `routes`: each row names 2 different experts. Within the rows of one index of ep (aligned blocks of 128 rows) no expert is named more than 40 times, a bound that some blocks reach.
All inputs are finite; a program needn't handle non-finite values.
Results may differ from a plain program's by a relative error of at most 0.025.
Values may be sent and summed in bfloat16 or wider, within the bound.
No kernel may reach another device: no remote copies, remote signals or barrier semaphores. Data moves between devices by JAX's collectives and lax.ppermute only.
A program may use at most 64 MiB of HBM per device.

v0:
```python
import jax
import jax.numpy as jnp
from jax import lax
from jax.sharding import PartitionSpec as P

HEADS = 16
KV_HEADS = 4
HEAD_DIM = 64
WINDOW = 128
TOP = 2


NORM_EPSILON = 1e-05
ROTARY_BASE = 500000.0
MASK_VALUE = -1e30


def padded(block, sides, width):
    for axis, dim in sides:
        count = lax.axis_size(axis)
        forward = [(i, i + 1) for i in range(count - 1)]
        backward = [(target, source) for source, target in forward]
        low = lax.ppermute(
            lax.slice_in_dim(block, block.shape[dim] - width, None, axis=dim), axis, forward
        )
        high = lax.ppermute(lax.slice_in_dim(block, 0, width, axis=dim), axis, backward)
        block = jnp.concatenate([low, block, high], axis=dim)
    return block


def layer_norm(activations, norm_gain):
    values = activations.astype(jnp.float32)
    average = jnp.mean(values, axis=-1, keepdims=True)
    centred = values - average
    variance = jnp.mean(centred * centred, axis=-1, keepdims=True)
    return (centred * lax.rsqrt(variance + NORM_EPSILON) * norm_gain).astype(jnp.bfloat16)


def rotate(head_rows, positions):
    half_dim = head_rows.shape[-1] // 2
    exponent = jnp.arange(half_dim, dtype=jnp.float32) * (2.0 / head_rows.shape[-1])
    frequency = jnp.power(jnp.float32(ROTARY_BASE), -exponent)
    angles = positions.astype(jnp.float32)[:, None] * frequency[None, :]
    cosine = jnp.cos(angles)[:, None, :]
    sine_part = jnp.sin(angles)[:, None, :]
    first_half = head_rows[..., :half_dim].astype(jnp.float32)
    second_half = head_rows[..., half_dim:].astype(jnp.float32)
    turned = jnp.concatenate(
        [
            first_half * cosine - second_half * sine_part,
            second_half * cosine + first_half * sine_part,
        ],
        axis=-1,
    )
    return turned.astype(jnp.bfloat16)


def on_device(
    queries,
    key_states,
    value_states,
    sink_logit,
    out_weight,
    expert_input,
    norm_gain,
    routes,
    route_weight,
    gate_weight,
    up_weight,
    down_weight,
):
    expert_devices = lax.axis_size("ep")
    group_devices = lax.axis_size("tp")
    expert_index = lax.axis_index("ep")
    tensor_index = lax.axis_index("tp")
    row_count = queries.shape[0]
    local_heads = queries.shape[1] // HEAD_DIM
    group_size = HEADS // KV_HEADS
    positions = expert_index * row_count + jnp.arange(row_count, dtype=jnp.int32)
    turned_query = rotate(queries.reshape(row_count, local_heads, HEAD_DIM), positions)
    shared_head = tensor_index * local_heads // group_size
    own_key = lax.dynamic_slice_in_dim(key_states, shared_head * HEAD_DIM, HEAD_DIM, 1)
    own_value = lax.dynamic_slice_in_dim(value_states, shared_head * HEAD_DIM, HEAD_DIM, 1)
    turned_key = rotate(own_key.reshape(row_count, 1, HEAD_DIM), positions).reshape(
        row_count, HEAD_DIM
    )
    key_value = jnp.concatenate([turned_key, own_value], axis=1)
    extended = padded(key_value, (("ep", 0),), WINDOW)
    span_keys = extended[:, :HEAD_DIM]
    span_values = extended[:, HEAD_DIM:]
    scores = jnp.einsum(
        "qhd,sd->hqs", turned_query, span_keys, preferred_element_type=jnp.float32
    ) * HEAD_DIM ** (-0.5)
    query_pos = positions[:, None]
    key_pos = (
        expert_index * row_count
        - WINDOW
        + jnp.arange(row_count + 2 * WINDOW, dtype=jnp.int32)[None, :]
    )
    allowed = (
        (jnp.abs(query_pos - key_pos) <= WINDOW)
        & (key_pos >= 0)
        & (key_pos < row_count * expert_devices)
    )
    scores = jnp.where(allowed[None, :, :], scores, MASK_VALUE)
    sinks = sink_logit[:, None, None]
    largest = jnp.maximum(jnp.max(scores, axis=-1, keepdims=True), sinks)
    weights = jnp.exp(scores - largest)
    denominator = jnp.sum(weights, axis=-1, keepdims=True) + jnp.exp(sinks - largest)
    probability = (weights / denominator).astype(jnp.bfloat16)
    attended = jnp.einsum(
        "hqs,sd->qhd", probability, span_values, preferred_element_type=jnp.float32
    )
    attended = attended.astype(jnp.bfloat16).reshape(row_count, local_heads * HEAD_DIM)
    mixer_out = lax.psum_scatter(
        jnp.dot(attended, out_weight, preferred_element_type=jnp.float32).astype(jnp.bfloat16),
        "tp",
        scatter_dimension=0,
        tiled=True,
    )
    token_count = expert_input.shape[0]
    expert_count = expert_devices * gate_weight.shape[0]
    capacity = token_count * TOP * 5 // (4 * expert_count)
    normed = layer_norm(expert_input, norm_gain)
    flat_routes = routes.reshape(-1)
    matches = (flat_routes[:, None] == jnp.arange(expert_count, dtype=jnp.int32)[None, :]).astype(
        jnp.int32
    )
    slot_rank = jnp.sum((jnp.cumsum(matches, axis=0) - matches) * matches, axis=1)
    slot_index = flat_routes * capacity + slot_rank
    slot_token = (
        jnp.zeros((expert_count * capacity,), jnp.int32)
        .at[slot_index]
        .set(jnp.arange(token_count * TOP, dtype=jnp.int32) // TOP)
    )
    matched = (
        slot_index.reshape(token_count, TOP)[None, :, :]
        == jnp.arange(expert_count * capacity, dtype=jnp.int32)[:, None, None]
    )
    combine = jnp.sum(
        jnp.where(
            matched, route_weight.astype(jnp.bfloat16)[None, :, :], jnp.zeros((), jnp.bfloat16)
        ),
        axis=2,
    )
    column_width = normed.shape[1] // group_devices
    own_columns = lax.dynamic_slice_in_dim(normed, tensor_index * column_width, column_width, 1)
    packed = jnp.take(own_columns, slot_token, axis=0)
    arrived = lax.all_to_all(packed, "ep", split_axis=0, concat_axis=0, tiled=True)
    portion = lax.all_gather(arrived, "tp", axis=1, tiled=True)
    gate_rows = gate_weight[0]
    up_rows = up_weight[0]
    gate_act = jnp.dot(portion, gate_rows, preferred_element_type=jnp.float32)
    up_act = jnp.dot(portion, up_rows, preferred_element_type=jnp.float32)
    hidden = (jax.nn.silu(gate_act) * up_act).astype(jnp.bfloat16)
    local_down = down_weight[0]
    summed = lax.psum_scatter(
        lax.dot_general(
            local_down, hidden, (((0,), (1,)), ((), ())), preferred_element_type=jnp.float32
        ).astype(jnp.bfloat16),
        "tp",
        scatter_dimension=0,
        tiled=True,
    )
    returned = lax.all_to_all(summed, "ep", split_axis=1, concat_axis=1, tiled=True)
    expert_out = lax.dot_general(
        combine, returned, (((0,), (1,)), ((), ())), preferred_element_type=jnp.float32
    ).astype(jnp.bfloat16)
    return (mixer_out, expert_out)


def solution(mesh):
    in_specs = (
        P("ep", "tp"),
        P("ep", None),
        P("ep", None),
        P("tp"),
        P("tp", None),
        P("ep", None),
        P(),
        P("ep", None),
        P("ep", None),
        P("ep", None, "tp"),
        P("ep", None, "tp"),
        P("ep", "tp", None),
    )
    out_specs = (P(("ep", "tp"), None), P("ep", "tp"))
    return jax.shard_map(
        on_device, mesh=mesh, in_specs=in_specs, out_specs=out_specs, check_vma=False
    )
```

profile of v0, /device:TPU:0, one launch (start us, length us, event | category | flops | bytes accessed | tf_op | source)
XLA Modules:
  0.0 121.7 jit_solution(18353182998390398198)
XLA Ops:
  7.2 0.0 copy-start
  7.2 0.0 copy-start.1
  7.2 0.0 all-gather.2.cloned.1.call-start
  7.2 0.9 copy.32
  8.1 0.1 eq.42
  8.3 0.1 eq.38
  8.4 0.6 reduce-window.6
  9.0 0.2 slice_reduce_fusion
  9.3 0.1 fusion.48
  9.4 0.1 reduce_sum.54
  9.6 0.1 mul.185
  9.7 1.4 %scatter_custom_fusion = s32[320]{0:T(512)S(1)} fusion(s32[256]{0:T(256)S(1)} %bitcast.70, s32[256]{0:T(256)S(1)} %and_select_fusion, s32[]{:T(128)} %constant.40.clone.1), kind=kCustom, calls=%fused_computation.84 | custom fusion | bytes 1284 | tf_op jit(solution)/shard_map/scatter | solution.py:134
  11.1 1.2 convert_reduce_fusion
  12.3 0.0 copy-done.1
  12.4 0.3 multiply_reduce_fusion
  12.7 0.1 broadcast_in_dim.67
  12.7 0.8 dynamic-slice
  13.5 0.1 fusion.26
  13.6 2.0 %gather_fusion = bf16[320,512]{1,0:T(8,128)(2,1)S(1)} fusion(bf16[128,512]{1,0:T(8,128)(2,1)S(1)} %fusion.26, s32[1024]{0:T(1024)S(1)} %pad_clamp_fusion), kind=kCustom, calls=%fused_computation | custom fusion | bytes 656640 | tf_op jit(solution)/shard_map/jit(_take)/gather | solution.py:148
  15.6 0.0 copy-start.3
  15.7 0.0 copy-start.4
  15.7 0.1 broadcast_select_fusion
  15.8 18.1 %all_to_all.21 = bf16[8,40,512]{2,1,0:T(8,128)(2,1)} all-to-all(bf16[8,40,512]{2,1,0:T(8,128)(2,1)S(1)} %broadcast_select_fusion), channel_id=1, replica_groups=mesh['ep'=8,'tp'=4] {'ep'}, dimensions={0} | all-to-all | bytes 655360 | tf_op jit(solution)/shard_map/all_to_all | solution.py:149
  33.9 0.0 all-gather.2.cloned.1.call-update
  33.9 0.0 reduce-scatter.5.cloned.1.call-start
  34.0 0.0 copy-done.3
  34.0 0.0 copy-done.4
  34.0 0.1 constant_dynamic-slice_fusion
  34.1 0.1 copy.28
  34.2 16.5 %all-gather.2.cloned.1.call-done = bf16[320,2048]{1,0:T(8,128)(2,1)} async-done(((bf16[320,512]{1,0:T(8,128)(2,1)}), bf16[320,2048]{1,0:T(8,128)(2,1)}) %all-gather.2.cloned.1.call-update) | async-done | bytes 1310736 | tf_op jit(solution)/shard_map/all_gather | solution.py:150
  50.7 0.0 copy-start.6
  50.7 5.3 %fusion.4 = f32[320,1024]{1,0:T(8,128)} fusion(bf16[320,2048]{1,0:T(8,128)(2,1)} %all-gather.2.cloned.1.call-done, bf16[1,2048,1024]{2,1,0:T(8,128)(2,1)} %param.21), kind=kOutput, calls=%fused_computation.6 | convolution fusion | flops 1342177280 | bytes 6815744 | tf_op jit(solution)/shard_map/dot_general | solution.py:153
  56.0 0.0 copy-done.6
  56.0 7.9 %fusion.9 = bf16[2048,320]{0,1:T(8,128)(2,1)} fusion(bf16[1,1024,2048]{2,1,0:T(8,128)(2,1)} %param.23, bf16[320,2048]{1,0:T(8,128)(2,1)S(1)} %copy-done.6, bf16[1,2048,1024]{2,1,0:T(8,128)(2,1)} %param.22, f32[320,1024]{1,0:T(8,128)} %fusion.4), kind=kOutput, calls=%fused_computation.9 | convolution fusion | flops 2686976000 | bytes 12320768 | tf_op jit(solution)/shard_map/dot_general | solution.py:158
  63.8 0.0 reduce-scatter.5.cloned.1.call-update
  63.9 0.0 reduce-scatter.3.cloned.1.call-start
  63.9 0.1 fusion.46
  64.1 0.1 copy.37
  64.2 3.4 %collective-permute-start = (bf16[128,128]{0,1:T(8,128)(2,1)S(1)}, bf16[128,128]{0,1:T(8,128)(2,1)S(1)}, u32[]{:S(2)}, u32[]{:S(2)}) collective-permute-start(bf16[128,128]{0,1:T(8,128)(2,1)S(1)} %pad_maximum_fusion.1), channel_id=1, source_target_pairs={{0,4},{4,8},{8,12},{12,16},{16,20},{20,24},{24,28},{1,5},{5,9},{9,... | collective-permute-start | bytes 98312 | tf_op jit(solution)/shard_map/ppermute | solution.py:23
  67.6 1.3 %collective-permute-start.1 = (bf16[128,128]{0,1:T(8,128)(2,1)S(1)}, bf16[128,128]{0,1:T(8,128)(2,1)S(1)}, u32[]{:S(2)}, u32[]{:S(2)}) collective-permute-start(bf16[128,128]{0,1:T(8,128)(2,1)S(1)} %pad_maximum_fusion.1), channel_id=1, source_target_pairs={{4,0},{8,4},{12,8},{16,12},{20,16},{24,20},{28,24},{5,1},{9,5},{13... | collective-permute-start | bytes 98312 | tf_op jit(solution)/shard_map/ppermute | solution.py:26
  68.9 0.0 copy-done.2
  68.9 0.1 copy.30
  69.0 0.1 multiply_cosine_fusion
  69.2 0.2 fusion.28
  69.4 0.0 collective-permute-done
  69.4 3.9 %collective-permute-done.1 = bf16[128,128]{0,1:T(8,128)(2,1)S(1)} collective-permute-done((bf16[128,128]{0,1:T(8,128)(2,1)S(1)}, bf16[128,128]{0,1:T(8,128)(2,1)S(1)}, u32[]{:S(2)}, u32[]{:S(2)}) %collective-permute-start.1) | collective-permute-done | bytes 32800 | tf_op jit(solution)/shard_map/ppermute | solution.py:26
  73.4 0.3 fusion.58
  73.7 0.0 copy-done.5
  73.7 0.1 broadcast_maximum_fusion
  73.8 0.1 fusion.22
  73.9 0.1 exponential_add_fusion
  74.0 0.3 convolution_convert_fusion.2
  74.3 0.0 copy-done
  74.3 0.0 copy-start.7
  74.3 1.2 convolution_convert_fusion
  75.4 0.0 reduce-scatter.3.cloned.1.call-update
  75.5 15.0 %reduce-scatter.5.cloned.1.call-done = bf16[512,320]{0,1:T(8,128)(2,1)} async-done(((bf16[2048,320]{0,1:T(8,128)(2,1)}), bf16[512,320]{0,1:T(8,128)(2,1)}) %reduce-scatter.5.cloned.1.call-update) | async-done | bytes 327696 | tf_op jit(solution)/shard_map/reduce_scatter | solution.py:157
  90.5 5.5 %all-to-all-start.1 = ((bf16[512,8,40]{0,2,1:T(8,128)(2,1)}), bf16[512,8,40]{0,2,1:T(8,128)(2,1)S(1)}, u32[]{:S(2)}, u32[]{:S(2)}) async-start(bf16[512,8,40]{0,2,1:T(8,128)(2,1)} %bitcast.65), calls=%async_computation.3 | async-start | bytes 655360 | tf_op jit(solution)/shard_map/all_to_all | solution.py:165
  96.0 0.1 copy.35
  96.0 0.0 copy-done.7
  96.0 0.1 fusion.29
  96.1 10.0 %all-to-all-done.1 = bf16[512,8,40]{0,2,1:T(8,128)(2,1)S(1)} async-done(((bf16[512,8,40]{0,2,1:T(8,128)(2,1)}), bf16[512,8,40]{0,2,1:T(8,128)(2,1)S(1)}, u32[]{:S(2)}, u32[]{:S(2)}) %all-to-all-start.1) | async-done | bytes 327712 | tf_op jit(solution)/shard_map/all_to_all | solution.py:165
  106.1 0.9 convolution_convert_fusion.1
  107.0 8.2 %reduce-scatter.3.cloned.1.call-done = bf16[32,2048]{1,0:T(8,128)(2,1)} async-done(((bf16[128,2048]{1,0:T(8,128)(2,1)}), bf16[32,2048]{1,0:T(8,128)(2,1)}) %reduce-scatter.3.cloned.1.call-update) | async-done | bytes 131088 | tf_op jit(solution)/shard_map/reduce_scatter | solution.py:115
  (22 shorter events, 0.2 us)
Async XLA Ops:
  7.2 67.1 %copy-start = (bf16[256,2048]{1,0:T(8,128)(2,1)S(1)}, bf16[256,2048]{1,0:T(8,128)(2,1)}, u32[]{:S(2)}) copy-start(bf16[256,2048]{1,0:T(8,128)(2,1)} %param.16) | copy-start | bytes 3145732
  7.2 5.2 %copy-start.1 = (bf16[128,2048]{1,0:T(8,128)(2,1)S(1)}, bf16[128,2048]{1,0:T(8,128)(2,1)}, u32[]{:S(2)}) copy-start(bf16[128,2048]{1,0:T(8,128)(2,1)} %param.17) | copy-start | bytes 1572868
  7.2 43.5 %all-gather.2.cloned.1.call-start = ((), (), s32[]{:S(2)}) async-start(), calls=%async_computation.5 | async-start | bytes 1638400 | tf_op jit(solution)/shard_map/all_gather | solution.py:150
  15.6 18.3 %copy-start.3 = (bf16[128,256]{1,0:T(8,128)(2,1)S(1)}, bf16[128,256]{1,0:T(8,128)(2,1)}, u32[]{:S(2)}) copy-start(bf16[128,256]{1,0:T(8,128)(2,1)} %param.14) | copy-start | bytes 196612
  15.7 18.3 %copy-start.4 = (bf16[128,256]{1,0:T(8,128)(2,1)S(1)}, bf16[128,256]{1,0:T(8,128)(2,1)}, u32[]{:S(2)}) copy-start(bf16[128,256]{1,0:T(8,128)(2,1)} %param.13) | copy-start | bytes 196612
  33.9 56.5 %reduce-scatter.5.cloned.1.call-start = ((), (), s32[]{:S(2)}) async-start(), calls=%async_computation.6 | async-start | bytes 1638400 | tf_op jit(solution)/shard_map/reduce_scatter | solution.py:157
  50.7 5.3 %copy-start.6 = (bf16[320,2048]{1,0:T(8,128)(2,1)S(1)}, bf16[320,2048]{1,0:T(8,128)(2,1)}, u32[]{:S(2)}) copy-start(bf16[320,2048]{1,0:T(8,128)(2,1)} %all-gather.2.cloned.1.call-done) | copy-start | bytes 3932164
  63.8 5.0 %copy-start.2 = (bf16[128,256]{1,0:T(8,128)(2,1)S(1)}, bf16[128,256]{1,0:T(8,128)(2,1)}, u32[]{:S(2)}) copy-start(bf16[128,256]{1,0:T(8,128)(2,1)} %param.12) | copy-start | bytes 196612
  63.8 9.8 %copy-start.5 = (f32[4]{0:T(128)S(1)}, f32[4]{0:T(128)}, u32[]{:S(2)}) copy-start(f32[4]{0:T(128)} %param.15) | copy-start | bytes 52
  63.9 51.3 %reduce-scatter.3.cloned.1.call-start = ((), (), s32[]{:S(2)}) async-start(), calls=%async_computation.4 | async-start | bytes 655360 | tf_op jit(solution)/shard_map/reduce_scatter | solution.py:115
  64.2 5.3 %collective-permute-start = (bf16[128,128]{0,1:T(8,128)(2,1)S(1)}, bf16[128,128]{0,1:T(8,128)(2,1)S(1)}, u32[]{:S(2)}, u32[]{:S(2)}) collective-permute-start(bf16[128,128]{0,1:T(8,128)(2,1)S(1)} %pad_maximum_fusion.1), channel_id=1, source_target_pairs={{0,4},{4,8},{8,12},{12,16},{16,20},{20,24},{24,28},{1,5},{5,9},{9,... | collective-permute-start | bytes 98312 | tf_op jit(solution)/shard_map/ppermute | solution.py:23
  67.6 5.8 %collective-permute-start.1 = (bf16[128,128]{0,1:T(8,128)(2,1)S(1)}, bf16[128,128]{0,1:T(8,128)(2,1)S(1)}, u32[]{:S(2)}, u32[]{:S(2)}) collective-permute-start(bf16[128,128]{0,1:T(8,128)(2,1)S(1)} %pad_maximum_fusion.1), channel_id=1, source_target_pairs={{4,0},{8,4},{12,8},{16,12},{20,16},{24,20},{28,24},{5,1},{9,5},{13... | collective-permute-start | bytes 98312 | tf_op jit(solution)/shard_map/ppermute | solution.py:26
  74.3 21.8 %copy-start.7 = (f32[128,2]{0,1:T(2,128)S(1)}, f32[128,2]{0,1:T(2,128)}, u32[]{:S(2)}) copy-start(f32[128,2]{0,1:T(2,128)} %param.20) | copy-start | bytes 3076
  90.5 15.7 %all-to-all-start.1 = ((bf16[512,8,40]{0,2,1:T(8,128)(2,1)}), bf16[512,8,40]{0,2,1:T(8,128)(2,1)S(1)}, u32[]{:S(2)}, u32[]{:S(2)}) async-start(bf16[512,8,40]{0,2,1:T(8,128)(2,1)} %bitcast.65), calls=%async_computation.3 | async-start | bytes 655360 | tf_op jit(solution)/shard_map/all_to_all | solution.py:165
Sparse Core Ops, SparseCore 0:
  34.0 16.5 all-gather.1
  64.0 26.4 reduce-scatter.4
  93.5 21.6 reduce-scatter.2
where the time goes:
time: 122 us
  waiting for transfers between devices  53.6 us (44%)
  blocking collectives  18.1 us (15%)
  matrix products  15.8 us (13%)
  between operations  14.1 us (12%)
  starting transfers between devices  10.3 us (8%)
  local copies, waits for them, and re-layouts  6.43 us (5%)
  other arithmetic  3.39 us (3%)
    all_to_all x1, blocking collectives, on_device(): lax.all_to_all(packed, 'ep', split_axis=0, concat_axis=0, tiled=True)  18.1 us
    all_gather x1, waiting for transfers between devices, on_device(): portion = lax.all_gather(arrived, 'tp', axis=1, tiled=True)  16.5 us
    reduce_scatter x1, waiting for transfers between devices, on_device(): lax.psum_scatter(lax.dot_general(local_down, hidden, (((0,), (1,)), ((),...  15 us
    all_to_all x1, waiting for transfers between devices, on_device(): lax.all_to_all(summed, 'ep', split_axis=1, concat_axis=1, tiled=True)  10 us
    reduce_scatter x1, waiting for transfers between devices, on_device(): lax.psum_scatter(jnp.dot(attended, out_weight, preferred_element_type=jnp...  8.2 us
    dot_general x1, matrix products, on_device(): lax.dot_general(local_down, hidden, (((0,), (1,)), ((), ())), preferred_e...  7.88 us
    all_to_all x1, starting transfers between devices, on_device(): lax.all_to_all(summed, 'ep', split_axis=1, concat_axis=1, tiled=True)  5.51 us
    dot_general x1, matrix products, on_device(): gate_act = jnp.dot(portion, gate_rows, preferred_element_type=jnp.float32)  5.29 us
  transfers between devices with their start and end apart: 6, of which 5 were waited for; matrix products, arithmetic and copies ran while one was open for 3% of the time, Pallas kernels for 0%

commit v1 on v0

v1 whole, which is shorter than its diff:
```python
import functools

import jax
import jax.numpy as jnp
from jax import lax
from jax.experimental import pallas as pl
from jax.experimental.pallas import tpu as pltpu
from jax.sharding import PartitionSpec as P

HEADS = 16
KV_HEADS = 4
HEAD_DIM = 64
WINDOW = 128
TOP = 2

NORM_EPSILON = 1e-05
ROTARY_BASE = 500000.0
MASK_VALUE = -1e30
LANES = 128
MIB = 1 << 20

VM = pl.BlockSpec(memory_space=pltpu.VMEM)
SM = pl.BlockSpec(memory_space=pltpu.SMEM)
ANY = pl.BlockSpec(memory_space=pl.ANY)
BF = jnp.bfloat16
F32 = jnp.float32


def call(body, out_shape, operands, in_specs, scratch=(), flops=0, nbytes=0, limit=24, out_specs=None, name=None):
    return pl.pallas_call(
        body,
        out_shape=out_shape,
        in_specs=in_specs,
        out_specs=out_specs if out_specs is not None else [VM] * len(out_shape),
        scratch_shapes=list(scratch),
        cost_estimate=pl.CostEstimate(flops=flops, bytes_accessed=nbytes, transcendentals=0),
        compiler_params=pltpu.CompilerParams(vmem_limit_bytes=limit * MIB),
        name=name,
    )(*operands)


def iota(shape, dim):
    return lax.broadcasted_iota(jnp.int32, shape, dim)


def strict_lower(n):
    return (iota((n, n), 0) > iota((n, n), 1)).astype(BF)


def matmul(a, b, dims=(((1,), (0,)), ((), ()))):
    return lax.dot_general(a, b, dims, preferred_element_type=F32)


def pack_body(cap, hops, group, place_ref, x_ref, gain_ref, routes_ref, key_ref, value_ref, kv_ref, *block_refs):
    ep_index, tp_index, head = place_ref[0], place_ref[1], place_ref[2]
    rows = x_ref.shape[0]
    keys, values = key_ref[...], value_ref[...]
    own_key = jnp.zeros((rows, HEAD_DIM), BF)
    own_value = jnp.zeros((rows, HEAD_DIM), BF)
    for h in range(keys.shape[1] // HEAD_DIM):
        own_key = jnp.where(head == h, keys[:, h * HEAD_DIM : (h + 1) * HEAD_DIM], own_key)
        own_value = jnp.where(head == h, values[:, h * HEAD_DIM : (h + 1) * HEAD_DIM], own_value)
    kv_ref[:, :HEAD_DIM] = own_key
    kv_ref[:, HEAD_DIM:] = own_value

    x = x_ref[...].astype(F32)
    average = jnp.mean(x, axis=-1, keepdims=True)
    centred = x - average
    variance = jnp.mean(centred * centred, axis=-1, keepdims=True)
    normed = (centred * lax.rsqrt(variance + NORM_EPSILON) * gain_ref[...]).astype(BF)

    pitch = LANES // hops
    column = iota((1, LANES), 1)
    hop, slot = column // pitch, column % pitch
    target = ep_index ^ (hop * group + tp_index)
    target = jnp.where(slot < cap, target, -1)
    hit = (routes_ref[:, 0:1] == target) | (routes_ref[:, 1:2] == target)
    rank = matmul(strict_lower(rows), hit.astype(BF))
    pick = jnp.where(hit & (rank.astype(jnp.int32) == slot), 1.0, 0.0)
    sent = matmul(jnp.transpose(pick).astype(BF), normed)
    for k, block_ref in enumerate(block_refs):
        block_ref[...] = sent[k * pitch : k * pitch + cap].astype(BF)


def mixer_body(
    cap, order, place_ref, q_ref, kv_ref, low_ref, high_ref, table_ref, sink_ref, routes_ref, rw_ref,
    wo_ref, wg_ref, wu_ref, wd_ref,
    send_ref, keep_ref, combine_ref, vg_ref, vu_ref, vd_ref, att_ref, sems,
):
    copies = [
        pltpu.make_async_copy(wg_ref, vg_ref, sems.at[0]),
        pltpu.make_async_copy(wu_ref, vu_ref, sems.at[1]),
        pltpu.make_async_copy(wd_ref, vd_ref, sems.at[2]),
    ]
    for c in copies:
        c.start()
    ep_index, tp_index = place_ref[0], place_ref[1]
    ep_count = place_ref[3]
    rows = q_ref.shape[0]
    span = rows + 2 * WINDOW
    heads = q_ref.shape[1] // HEAD_DIM
    half = HEAD_DIM // 2
    swap = (iota((HEAD_DIM, HEAD_DIM), 0) == (iota((HEAD_DIM, HEAD_DIM), 1) + half) % HEAD_DIM).astype(BF)
    table = table_ref[...]
    cosine, sine = table[:, :HEAD_DIM], table[:, HEAD_DIM:]
    kv = jnp.concatenate([low_ref[...], kv_ref[...], high_ref[...]], axis=0)
    raw_key, span_value = kv[:, :HEAD_DIM], kv[:, HEAD_DIM:]
    span_key = (raw_key.astype(F32) * cosine + matmul(raw_key, swap) * sine).astype(BF)
    own_cosine, own_sine = cosine[WINDOW : WINDOW + rows], sine[WINDOW : WINDOW + rows]
    distance = iota((rows, span), 1) - WINDOW - iota((rows, span), 0)
    key_pos = ep_index * rows - WINDOW + iota((rows, span), 1)
    allowed = (jnp.abs(distance) <= WINDOW) & (key_pos >= 0) & (key_pos < rows * ep_count)
    for h in range(heads):
        q = q_ref[:, h * HEAD_DIM : (h + 1) * HEAD_DIM]
        q = (q.astype(F32) * own_cosine + matmul(q, swap) * own_sine).astype(BF)
        scores = matmul(q, span_key, (((1,), (1,)), ((), ()))) * HEAD_DIM ** (-0.5)
        scores = jnp.where(allowed, scores, MASK_VALUE)
        sink = sink_ref[h]
        largest = jnp.maximum(jnp.max(scores, axis=-1, keepdims=True), sink)
        weights = jnp.exp(scores - largest)
        total = jnp.sum(weights, axis=-1, keepdims=True) + jnp.exp(sink - largest)
        probability = (weights / total).astype(BF)
        att_ref[:, h * HEAD_DIM : (h + 1) * HEAD_DIM] = matmul(probability, span_value)
    share = rows // len(order)
    piece = lambda n: att_ref[pl.ds(pl.multiple_of((tp_index ^ n) * share, share), share), :]
    ordered = jnp.concatenate([piece(n) for n in order], axis=0).astype(BF)
    partial = matmul(ordered, wo_ref[...]).astype(BF)
    keep_ref[...] = partial[: rows // 2]
    send_ref[...] = partial[rows // 2 :]

    slots = combine_ref.shape[1]
    column = iota((1, slots), 1)
    expert, slot = column // cap, column % cap
    hit0 = routes_ref[:, 0:1] == expert
    hit1 = routes_ref[:, 1:2] == expert
    rank = matmul(strict_lower(rows), (hit0 | hit1).astype(BF)).astype(jnp.int32)
    here = rank == slot
    weight = jnp.where(hit0 & here, rw_ref[:, 0:1], 0.0) + jnp.where(hit1 & here, rw_ref[:, 1:2], 0.0)
    combine_ref[...] = weight.astype(BF)
    for c in copies:
        c.wait()


def swapped_rows(value, cap, tp, bit):
    blocks = value.shape[0] // cap
    take = lambda i: value[(i ^ bit) * cap : (i ^ bit) * cap + cap]
    return jnp.concatenate([take(i) for i in range(blocks)], axis=0)


def expert_body(cap, order, place_ref, *refs):
    tp_index = place_ref[1]
    count = len(refs) - 8
    block_refs = refs[:count]
    wg_ref, wu_ref, wd_ref, send_ref, keep_ref, x_ref, h_ref, hs_ref = refs[count:]
    for i, block_ref in enumerate(block_refs):
        x_ref[i * cap : (i + 1) * cap, :] = block_ref[...]
    units = wg_ref.shape[1]
    tile = min(256, units)

    def hidden(i, _):
        at = pl.ds(pl.multiple_of(i * tile, tile), tile)
        x = x_ref[...]
        gate = matmul(x, wg_ref[:, at])
        up = matmul(x, wu_ref[:, at])
        value = gate / (1.0 + jnp.exp(-gate)) * up
        h_ref[:, at] = value.astype(BF)
        hs_ref[:, at] = swapped_rows(value, cap, len(order), 1).astype(BF)
        return 0

    lax.fori_loop(0, units // tile, hidden, 0)
    slice_width = wd_ref.shape[1] // len(order)
    kept = len(order) // 2
    width = min(256, slice_width)
    parts = slice_width // width
    for i, n in enumerate(order):
        base = (tp_index ^ n) * slice_width
        lhs_ref, out_ref = (h_ref, keep_ref) if i < kept else (hs_ref, send_ref)
        for j in range(parts):
            at = pl.ds(pl.multiple_of(base + j * width, width), width)
            column = (i % kept) * slice_width + j * width
            out_ref[:, column : column + width] = matmul(lhs_ref[...], wd_ref[:, at]).astype(BF)


def half_body(cap, tp, bit, keep_ref, got_ref, next_keep_ref, next_send_ref):
    middle = keep_ref.shape[1] // 2
    total = keep_ref[...].astype(F32) + got_ref[...].astype(F32)
    next_keep_ref[...] = total[:, :middle].astype(BF)
    next_send_ref[...] = swapped_rows(total[:, middle:], cap, tp, bit).astype(BF)


def last_body(cap, tp, place_ref, keep_ref, got_ref, out_ref):
    ep_index, tp_index = place_ref[0], place_ref[1]
    total = (keep_ref[...].astype(F32) + got_ref[...].astype(F32)).astype(BF)
    for i in range(total.shape[0] // cap):
        k, m = i // tp, i % tp
        out_ref[ep_index ^ (k * tp + (tp_index ^ m))] = total[i * cap : (i + 1) * cap]


def combine_body(combine_ref, rows_ref, out_ref):
    out_ref[...] = matmul(combine_ref[...], rows_ref[...]).astype(BF)


def halves_order(tp):
    bits = tp.bit_length() - 1
    return sorted(range(tp), key=lambda n: [n >> b & 1 for b in range(bits)])


def swap_pairs(count, bit):
    return [(i, i ^ bit) for i in range(count)]


def on_device(
    queries,
    key_states,
    value_states,
    sink_logit,
    out_weight,
    expert_input,
    norm_gain,
    routes,
    route_weight,
    gate_weight,
    up_weight,
    down_weight,
):
    ep, tp = lax.axis_size("ep"), lax.axis_size("tp")
    ep_index, tp_index = lax.axis_index("ep"), lax.axis_index("tp")
    rows, width = expert_input.shape
    local_heads = queries.shape[1] // HEAD_DIM
    group_size = HEADS // KV_HEADS
    expert_count = ep * gate_weight.shape[0]
    cap = rows * TOP * 5 // (4 * expert_count)
    slots = expert_count * cap
    hops = ep // tp
    order = halves_order(tp)
    units = gate_weight.shape[2]
    place = jnp.stack([ep_index, tp_index, tp_index * local_heads // group_size, ep]).astype(jnp.int32)
    block = jax.ShapeDtypeStruct((cap, width), BF)

    kv, *blocks = call(
        functools.partial(pack_body, cap, hops, tp),
        [jax.ShapeDtypeStruct((rows, 2 * HEAD_DIM), BF)] + [block] * hops,
        (place, expert_input, norm_gain.reshape(1, width), routes, key_states, value_states),
        [SM] + [VM] * 5,
        flops=2 * LANES * LANES * width,
        nbytes=rows * width * 2,
        name="pack",
    )

    held = {}
    for k in reversed(range(hops)):
        pairs = [(e * tp + t, (e ^ (k * tp + t)) * tp + t) for e in range(ep) for t in range(tp)]
        held[k, 0] = lax.ppermute(blocks[k], ("ep", "tp"), pairs)
    up_pairs = [(i, i + 1) for i in range(ep - 1)]
    down_pairs = [(i + 1, i) for i in range(ep - 1)]
    low = lax.ppermute(kv, "ep", up_pairs)
    high = lax.ppermute(kv, "ep", down_pairs)

    half = HEAD_DIM // 2
    frequency = jnp.power(F32(ROTARY_BASE), -(jnp.arange(half, dtype=F32) * (2.0 / HEAD_DIM)))
    span_pos = ep_index * rows - WINDOW + jnp.arange(rows + 2 * WINDOW, dtype=jnp.int32)
    angles = span_pos.astype(F32)[:, None] * frequency[None, :]
    cosine, sine = jnp.cos(angles), jnp.sin(angles)
    table = jnp.concatenate([cosine, cosine, -sine, sine], axis=1)

    gate_rows, up_rows, down_rows = gate_weight[0], up_weight[0], down_weight[0]
    shape = lambda a: jax.ShapeDtypeStruct(a.shape, a.dtype)
    half_rows = jax.ShapeDtypeStruct((rows // 2, width), BF)
    mix_send, mix_keep, combine, gate_v, up_v, down_v = call(
        functools.partial(mixer_body, cap, order),
        [half_rows, half_rows, jax.ShapeDtypeStruct((rows, slots), BF)]
        + [pltpu.VMEM(a.shape, a.dtype) for a in (gate_rows, up_rows, down_rows)],
        (place, queries, kv, low, high, table, sink_logit, routes, route_weight, out_weight, gate_rows, up_rows, down_rows),
        [SM] + [VM] * 5 + [SM] + [VM] * 3 + [ANY] * 3,
        scratch=[pltpu.VMEM((rows, local_heads * HEAD_DIM), F32), pltpu.SemaphoreType.DMA((3,))],
        flops=4 * rows * width * local_heads * HEAD_DIM,
        nbytes=3 * units * width * 2,
        limit=36,
        name="mixer",
    )

    bit = tp // 2
    while bit:
        for k in reversed(range(hops)):
            for m in [m for kk, m in held if kk == k]:
                held[k, m ^ bit] = lax.ppermute(held[k, m], "tp", swap_pairs(tp, bit))
        bit //= 2

    send, keep = call(
        functools.partial(expert_body, cap, order),
        [jax.ShapeDtypeStruct((slots, width // 2), BF)] * 2,
        (place, *[held[k, m] for k in range(hops) for m in range(tp)], gate_v, up_v, down_v),
        [SM] + [VM] * (hops * tp + 3),
        scratch=[pltpu.VMEM((slots, width), BF), pltpu.VMEM((slots, units), BF), pltpu.VMEM((slots, units), BF)],
        flops=6 * slots * width * units,
        nbytes=slots * width * 4,
        limit=36,
        name="expert",
    )

    bit = 1
    while bit < tp:
        got = lax.ppermute(send, "tp", swap_pairs(tp, bit))
        mix_got = lax.ppermute(mix_send, "tp", swap_pairs(tp, bit))
        mix = (mix_keep.astype(F32) + mix_got.astype(F32)).astype(BF)
        if bit * 2 < tp:
            middle = keep.shape[1] // 2
            keep, send = call(
                functools.partial(half_body, cap, tp, bit * 2),
                [jax.ShapeDtypeStruct((slots, middle), BF)] * 2,
                (keep, got),
                [VM] * 2,
                flops=slots * middle,
                nbytes=slots * middle * 8,
                name="half",
            )
            mix_keep, mix_send = mix[: mix.shape[0] // 2], mix[mix.shape[0] // 2 :]
        bit *= 2
    (ready,) = call(
        functools.partial(last_body, cap, tp),
        [jax.ShapeDtypeStruct((ep, cap, width // tp), BF)],
        (place, keep, got),
        [SM, VM, VM],
        flops=slots * width // tp,
        nbytes=slots * width // tp * 6,
        name="last",
    )
    returned = lax.all_to_all(ready, "ep", split_axis=0, concat_axis=0, tiled=True)
    (expert_out,) = call(
        combine_body,
        [jax.ShapeDtypeStruct((rows, width // tp), BF)],
        (combine, returned.reshape(slots, width // tp)),
        [VM, VM],
        flops=2 * slots * rows * width // tp,
        nbytes=slots * width // tp * 2,
        name="combine",
    )
    return (mix, expert_out)


def solution(mesh):
    in_specs = (
        P("ep", "tp"),
        P("ep", None),
        P("ep", None),
        P("tp"),
        P("tp", None),
        P("ep", None),
        P(),
        P("ep", None),
        P("ep", None),
        P("ep", None, "tp"),
        P("ep", None, "tp"),
        P("ep", "tp", None),
    )
    out_specs = (P(("ep", "tp"), None), P("ep", "tp"))
    return jax.shard_map(
        on_device, mesh=mesh, in_specs=in_specs, out_specs=out_specs, check_vma=False
    )
```

time: 122 us -> 79.3 us (0.65)
  waiting for transfers between devices: 53.6 us -> 24.6 us
  blocking collectives: 18.1 us -> 0 us
  starting transfers between devices: 10.3 us -> 28 us
  matrix products: 15.8 us -> 0 us
  Pallas kernels: 0 us -> 15.7 us
  between operations: 14.1 us -> 0.81 us
  other arithmetic: 3.39 us -> 1.83 us
  local copies, waits for them, and re-layouts: 6.43 us -> 7.72 us
    reduce_scatter x2 -> x0, waiting for transfers between devices: 23.2 us -> none  [the longest x1 15 us: on_device(): lax.psum_scatter(lax.dot_general(local_down, hidden, (((0,), (1,)), ((),...]
    all_to_all x1 -> x0, blocking collectives: 18.1 us -> none  [on_device(): lax.all_to_all(packed, 'ep', split_axis=0, concat_axis=0, tiled=True)]
    ppermute x2 -> x14, starting transfers between devices: 4.67 us -> 22 us  [the longest x6 9.83 us: on_device(): held[k, m ^ bit] = lax.ppermute(held[k, m], 'tp', swap_pairs(tp, bit))]
    all_gather x1 -> x0, waiting for transfers between devices: 16.5 us -> none  [on_device(): portion = lax.all_gather(arrived, 'tp', axis=1, tiled=True)]
    dot_general x6 -> x0, matrix products: 15.8 us -> none  [the longest x1 7.88 us: on_device(): lax.dot_general(local_down, hidden, (((0,), (1,)), ((), ())), preferred_e...]
    pallas_call x0 -> x6, Pallas kernels: none -> 15.7 us  [call(): pl.pallas_call(body, out_shape=out_shape, in_specs=in_specs, out_specs=ou...]
    ppermute x2 -> x14, waiting for transfers between devices: 3.93 us -> 16.4 us  [the longest x2 9.99 us: on_device(): got = lax.ppermute(send, 'tp', swap_pairs(tp, bit))]
    unnamed x19 -> x16, local copies, waits for them, and re-layouts: 1.15 us -> 7.71 us
  transfers between devices with their start and end apart: 6 -> 15, of which waited for: 5 -> 5; matrix products, arithmetic and copies ran while one was open for 3% -> 3% of each run, Pallas kernels for 0% -> 10%
where the time goes in v1:
time: 79.3 us; the launch traced here: 78.7 us
  starting transfers between devices  28 us (35%)
  waiting for transfers between devices  24.6 us (31%)
  Pallas kernels  15.7 us (20%)
  local copies, waits for them, and re-layouts  7.72 us (10%)
  other arithmetic  1.83 us (2%)
  between operations  0.81 us (1%)
    pallas_call x6, Pallas kernels, call(): pl.pallas_call(body, out_shape=out_shape, in_specs=in_specs, out_specs=ou...  15.7 us
    ppermute x2, waiting for transfers between devices, on_device(): got = lax.ppermute(send, 'tp', swap_pairs(tp, bit))  9.99 us
    ppermute x6, starting transfers between devices, on_device(): held[k, m ^ bit] = lax.ppermute(held[k, m], 'tp', swap_pairs(tp, bit))  9.83 us
    all_to_all x1, waiting for transfers between devices, on_device(): lax.all_to_all(ready, 'ep', split_axis=0, concat_axis=0, tiled=True)  8.22 us
    unnamed x16, local copies, waits for them, and re-layouts  7.71 us
    all_to_all x1, starting transfers between devices, on_device(): lax.all_to_all(ready, 'ep', split_axis=0, concat_axis=0, tiled=True)  5.97 us
    ppermute x2, starting transfers between devices, on_device(): held[k, 0] = lax.ppermute(blocks[k], ('ep', 'tp'), pairs)  4.8 us
    ppermute x1, waiting for transfers between devices, on_device(): high = lax.ppermute(kv, 'ep', down_pairs)  3.79 us
  transfers between devices with their start and end apart: 15, of which 5 were waited for; matrix products, arithmetic and copies ran while one was open for 3% of the time, Pallas kernels for 10%

profile of v1, /device:TPU:0, one launch (start us, length us, event | category | flops | bytes accessed | tf_op | source)
XLA Modules:
  0.0 78.7 jit_solution(16395367386032801884)
XLA Ops:
  0.6 0.8 copy.17.routes_ref
  1.4 0.1 pad_add_fusion.place_ref
  1.5 0.0 copy-start.1
  1.5 1.0 %copy-done.1 = bf16[128,2048]{1,0:T(8,128)(2,1)S(1)} copy-done((bf16[128,2048]{1,0:T(8,128)(2,1)S(1)}, bf16[128,2048]{1,0:T(8,128)(2,1)}, u32[]{:S(2)}) %copy-start.1) | copy-done | bytes 524312
  2.6 0.0 copy-start.3
  2.6 0.8 %copy-done.3 = bf16[128,256]{1,0:T(8,128)(2,1)S(1)} copy-done((bf16[128,256]{1,0:T(8,128)(2,1)S(1)}, bf16[128,256]{1,0:T(8,128)(2,1)}, u32[]{:S(2)}) %copy-start.3) | copy-done | bytes 65560
  3.4 0.0 copy-start.4
  3.4 0.8 %copy-done.4 = bf16[128,256]{1,0:T(8,128)(2,1)S(1)} copy-done((bf16[128,256]{1,0:T(8,128)(2,1)S(1)}, bf16[128,256]{1,0:T(8,128)(2,1)}, u32[]{:S(2)}) %copy-start.4) | copy-done | bytes 65560
  4.2 0.0 copy-start.5
  4.2 0.7 copy-done.5
  4.9 1.2 %pack.1 = (bf16[128,128]{1,0:T(8,128)(2,1)S(1)}, bf16[40,2048]{1,0:T(8,128)(2,1)S(1)}, bf16[40,2048]{1,0:T(8,128)(2,1)S(1)}) custom-call(s32[4]{0:T(128)S(1)} %pad_add_fusion.place_ref, bf16[128,2048]{1,0:T(8,128)(2,1)S(1)} %copy-done.1, f32[1,2048]{1,0:T(1,128)S(1)} %bitcast.9, s32[128,2]{1,0:T(8,128)S(1)} %copy.17.routes_ref, ...), custom_call_target="tpu_custom_call" | custom-call | flops 67108864 | bytes 524288 | tf_op jit(solution)/shard_map/pack/pallas_call | solution.py:30
  6.1 0.7 collective-permute-start.4
  6.8 4.1 %collective-permute-start.8 = (bf16[40,2048]{1,0:T(8,128)(2,1)S(1)}, bf16[40,2048]{1,0:T(8,128)(2,1)S(1)}, u32[]{:S(2)}, u32[]{:S(2)}) collective-permute-start(bf16[40,2048]{1,0:T(8,128)(2,1)S(1)} %get-tuple-element.20), channel_id=1, source_target_pairs={{0,16},{1,21},{2,26},{3,31},{4,20},{5,17},{6,30},{7,27},{8,24},{9,... | collective-permute-start | bytes 491528 | tf_op jit(solution)/shard_map/ppermute | solution.py:253
  11.0 3.4 %collective-permute-start = (bf16[128,128]{1,0:T(8,128)(2,1)S(1)}, bf16[128,128]{1,0:T(8,128)(2,1)S(1)}, u32[]{:S(2)}, u32[]{:S(2)}) collective-permute-start(bf16[128,128]{1,0:T(8,128)(2,1)S(1)} %get-tuple-element.15.kv_ref), channel_id=1, source_target_pairs={{0,4},{4,8},{8,12},{12,16},{16,20},{20,24},{24,28},{1,5},{5,9},{9,... | collective-permute-start | bytes 98312 | tf_op jit(solution)/shard_map/ppermute | solution.py:256
  14.4 0.0 collective-permute-done.4.refs_0_
  14.4 4.3 %collective-permute-start.6 = (bf16[40,2048]{1,0:T(8,128)(2,1)S(1)}, bf16[40,2048]{1,0:T(8,128)(2,1)S(1)}, u32[]{:S(2)}, u32[]{:S(2)}) collective-permute-start(bf16[40,2048]{1,0:T(8,128)(2,1)S(1)} %collective-permute-done.4.refs_0_), channel_id=1, source_target_pairs={{0,2},{1,3},{2,0},{3,1},{4,6},{5,7},{6,4},{7,5},{8,10},{9,11},{10,... | collective-permute-start | bytes 491528 | tf_op jit(solution)/shard_map/ppermute | solution.py:286
  18.6 0.0 collective-permute-done.8.refs_4_
  18.6 4.9 %collective-permute-start.10 = (bf16[40,2048]{1,0:T(8,128)(2,1)S(1)}, bf16[40,2048]{1,0:T(8,128)(2,1)S(1)}, u32[]{:S(2)}, u32[]{:S(2)}) collective-permute-start(bf16[40,2048]{1,0:T(8,128)(2,1)S(1)} %collective-permute-done.8.refs_4_), channel_id=1, source_target_pairs={{0,2},{1,3},{2,0},{3,1},{4,6},{5,7},{6,4},{7,5},{8,10},{9,11},{10,... | collective-permute-start | bytes 491528 | tf_op jit(solution)/shard_map/ppermute | solution.py:286
  23.6 0.1 collective-permute-start.5
  23.6 0.5 collective-permute-start.9
  24.1 0.0 collective-permute-done.6.refs_2_
  24.1 0.1 collective-permute-start.7
  24.2 2.6 %collective-permute-done.10.refs_6_ = bf16[40,2048]{1,0:T(8,128)(2,1)S(1)} collective-permute-done((bf16[40,2048]{1,0:T(8,128)(2,1)S(1)}, bf16[40,2048]{1,0:T(8,128)(2,1)S(1)}, u32[]{:S(2)}, u32[]{:S(2)}) %collective-permute-start.10) | collective-permute-done | bytes 163872 | tf_op jit(solution)/shard_map/ppermute | solution.py:286
  26.8 0.0 collective-permute-start.11
  26.8 0.8 multiply_cosine_fusion
  27.6 0.0 collective-permute-done.low_ref
  27.6 1.3 %collective-permute-start.1 = (bf16[128,128]{1,0:T(8,128)(2,1)S(1)}, bf16[128,128]{1,0:T(8,128)(2,1)S(1)}, u32[]{:S(2)}, u32[]{:S(2)}) collective-permute-start(bf16[128,128]{1,0:T(8,128)(2,1)S(1)} %get-tuple-element.15.kv_ref), channel_id=1, source_target_pairs={{4,0},{8,4},{12,8},{16,12},{20,16},{24,20},{28,24},{5,1},{9,5},{13... | collective-permute-start | bytes 98312 | tf_op jit(solution)/shard_map/ppermute | solution.py:257
  28.9 0.2 pad_maximum_fusion.table_ref
  29.2 0.8 %copy.20.rw_ref = f32[128,2]{1,0:T(8,128)S(1)} copy(f32[128,2]{0,1:T(2,128)} %param.20) | data formatting | bytes 2048 | tf_op args[8]
  29.9 3.8 %collective-permute-done.1.high_ref = bf16[128,128]{1,0:T(8,128)(2,1)S(1)} collective-permute-done((bf16[128,128]{1,0:T(8,128)(2,1)S(1)}, bf16[128,128]{1,0:T(8,128)(2,1)S(1)}, u32[]{:S(2)}, u32[]{:S(2)}) %collective-permute-start.1) | collective-permute-done | bytes 32800 | tf_op jit(solution)/shard_map/ppermute | solution.py:257
  33.7 0.0 copy-start
  33.7 1.2 %copy-done = bf16[256,2048]{1,0:T(8,128)(2,1)S(1)} copy-done((bf16[256,2048]{1,0:T(8,128)(2,1)S(1)}, bf16[256,2048]{1,0:T(8,128)(2,1)}, u32[]{:S(2)}) %copy-start) | copy-done | bytes 1048600
  35.0 0.0 copy-start.2
  35.0 0.8 %copy-done.2 = bf16[128,256]{1,0:T(8,128)(2,1)S(1)} copy-done((bf16[128,256]{1,0:T(8,128)(2,1)S(1)}, bf16[128,256]{1,0:T(8,128)(2,1)}, u32[]{:S(2)}) %copy-start.2) | copy-done | bytes 65560
  35.8 0.0 copy-start.6
  35.8 0.7 copy-done.6
  36.5 6.4 %mixer.1 = (bf16[64,2048]{1,0:T(8,128)(2,1)S(1)}, bf16[64,2048]{1,0:T(8,128)(2,1)S(1)}, bf16[128,320]{1,0:T(8,128)(2,1)S(1)}, bf16[2048,1024]{1,0:T(8,128)(2,1)S...) custom-call(s32[4]{0:T(128)S(1)} %pad_add_fusion.place_ref, bf16[128,256]{1,0:T(8,128)(2,1)S(1)} %copy-done.2, ...), custom_call_target="tpu_custom_call" | custom-call | flops 268435456 | bytes 12582912 | tf_op jit(solution)/shard_map/mixer/pallas_call | solution.py:30
  42.9 0.0 collective-permute-done.5.refs_1_
  42.9 0.0 collective-permute-done.9.refs_5_
  42.9 0.0 collective-permute-done.7.refs_3_
  42.9 0.0 collective-permute-done.11.refs_7_
  42.9 5.7 %expert.1 = (bf16[320,1024]{1,0:T(8,128)(2,1)S(1)}, bf16[320,1024]{1,0:T(8,128)(2,1)S(1)}) custom-call(s32[4]{0:T(128)S(1)} %pad_add_fusion.place_ref, bf16[40,2048]{1,0:T(8,128)(2,1)S(1)} %collective-permute-done.4.refs_0_, bf16[40,2048]{1,0:T(8,128)(2,1)S(1)} %collective-permute-done.5.refs_1_, bf16[40,2048]{1,0:T(8,128)(2,1)S(1)} %collective-permute-done.6.refs_2_, ...), custom_call_target="tpu_custom_call" | custom-call | flops 4026531840 | bytes 2621440 | tf_op jit(solution)/shard_map/expert/pallas_call | solution.py:30
  48.6 0.1 collective-permute-start.12
  48.7 0.5 collective-permute-start.2
  49.2 1.6 %collective-permute-done.12.got_ref = bf16[320,1024]{1,0:T(8,128)(2,1)S(1)} collective-permute-done((bf16[320,1024]{1,0:T(8,128)(2,1)S(1)}, bf16[320,1024]{1,0:T(8,128)(2,1)S(1)}, u32[]{:S(2)}, u32[]{:S(2)}) %collective-permute-start.12) | collective-permute-done | bytes 655392 | tf_op jit(solution)/shard_map/ppermute | solution.py:303
  50.8 0.2 half.1
  51.0 1.8 %collective-permute-start.13 = (bf16[320,512]{1,0:T(8,128)(2,1)S(1)}, bf16[320,512]{1,0:T(8,128)(2,1)S(1)}, u32[]{:S(2)}, u32[]{:S(2)}) collective-permute-start(bf16[320,512]{1,0:T(8,128)(2,1)S(1)} %get-tuple-element.27), channel_id=1, source_target_pairs={{0,2},{1,3},{2,0},{3,1},{4,6},{5,7},{6,4},{7,5},{8,10},{9,11},{10,... | collective-permute-start | bytes 983048 | tf_op jit(solution)/shard_map/ppermute | solution.py:303
  52.8 0.0 collective-permute-done.2
  52.8 0.1 add_convert_fusion
  52.9 0.4 collective-permute-start.3
  53.2 8.4 %collective-permute-done.13.got_ref = bf16[320,512]{1,0:T(8,128)(2,1)S(1)} collective-permute-done((bf16[320,512]{1,0:T(8,128)(2,1)S(1)}, bf16[320,512]{1,0:T(8,128)(2,1)S(1)}, u32[]{:S(2)}, u32[]{:S(2)}) %collective-permute-start.13) | collective-permute-done | bytes 327712 | tf_op jit(solution)/shard_map/ppermute | solution.py:303
  61.6 1.3 %last.1 = bf16[8,40,512]{2,1,0:T(8,128)(2,1)} custom-call(s32[4]{0:T(128)S(1)} %pad_add_fusion.place_ref, bf16[320,512]{1,0:T(8,128)(2,1)S(1)} %get-tuple-element.26.keep_ref, bf16[320,512]{1,0:T(8,128)(2,1)S(1)} %collective-permute-done.13.got_ref), custom_call_target="tpu_custom_call" | custom-call | flops 163840 | bytes 983040 | tf_op jit(solution)/shard_map/last/pallas_call | solution.py:30
  63.0 6.0 %all-to-all-start = ((bf16[8,40,512]{2,1,0:T(8,128)(2,1)}), bf16[8,40,512]{2,1,0:T(8,128)(2,1)S(1)}, u32[]{:S(2)}, u32[]{:S(2)}) async-start(bf16[8,40,512]{2,1,0:T(8,128)(2,1)} %last.1), calls=%async_computation | async-start | bytes 655360 | tf_op jit(solution)/shard_map/all_to_all | solution.py:328
  68.9 0.0 collective-permute-done.3
  68.9 0.7 add_convert_fusion.1
  69.6 8.2 %all-to-all-done = bf16[8,40,512]{2,1,0:T(8,128)(2,1)S(1)} async-done(((bf16[8,40,512]{2,1,0:T(8,128)(2,1)}), bf16[8,40,512]{2,1,0:T(8,128)(2,1)S(1)}, u32[]{:S(2)}, u32[]{:S(2)}) %all-to-all-start) | async-done | bytes 327712 | tf_op jit(solution)/shard_map/all_to_all | solution.py:328
  77.9 0.9 %combine.1 = bf16[128,512]{1,0:T(8,128)(2,1)} custom-call(bf16[128,320]{1,0:T(8,128)(2,1)S(1)} %get-tuple-element.18.combine_ref, bf16[320,512]{1,0:T(8,128)(2,1)S(1)} %bitcast.8), custom_call_target="tpu_custom_call" | custom-call | flops 41943040 | bytes 327680 | tf_op jit(solution)/shard_map/combine/pallas_call | solution.py:30
  (3 shorter events, 0.0 us)
Async XLA Ops:
  1.5 1.0 %copy-start.1 = (bf16[128,2048]{1,0:T(8,128)(2,1)S(1)}, bf16[128,2048]{1,0:T(8,128)(2,1)}, u32[]{:S(2)}) copy-start(bf16[128,2048]{1,0:T(8,128)(2,1)} %x_ref.1) | copy-start | bytes 1572868
  2.6 0.8 %copy-start.3 = (bf16[128,256]{1,0:T(8,128)(2,1)S(1)}, bf16[128,256]{1,0:T(8,128)(2,1)}, u32[]{:S(2)}) copy-start(bf16[128,256]{1,0:T(8,128)(2,1)} %key_ref.1) | copy-start | bytes 196612
  3.4 0.8 %copy-start.4 = (bf16[128,256]{1,0:T(8,128)(2,1)S(1)}, bf16[128,256]{1,0:T(8,128)(2,1)}, u32[]{:S(2)}) copy-start(bf16[128,256]{1,0:T(8,128)(2,1)} %value_ref.1) | copy-start | bytes 196612
  4.2 0.7 copy-start.5
  6.1 8.2 %collective-permute-start.4 = (bf16[40,2048]{1,0:T(8,128)(2,1)S(1)}, bf16[40,2048]{1,0:T(8,128)(2,1)S(1)}, u32[]{:S(2)}, u32[]{:S(2)}) collective-permute-start(bf16[40,2048]{1,0:T(8,128)(2,1)S(1)} %get-tuple-element.19), channel_id=1, source_target_pairs={{0,0},{1,5},{2,10},{3,15},{4,4},{5,1},{6,14},{7,11},{8,8},{9,13},{... | collective-permute-start | bytes 491528 | tf_op jit(solution)/shard_map/ppermute | solution.py:253
  6.8 11.8 %collective-permute-start.8 = (bf16[40,2048]{1,0:T(8,128)(2,1)S(1)}, bf16[40,2048]{1,0:T(8,128)(2,1)S(1)}, u32[]{:S(2)}, u32[]{:S(2)}) collective-permute-start(bf16[40,2048]{1,0:T(8,128)(2,1)S(1)} %get-tuple-element.20), channel_id=1, source_target_pairs={{0,16},{1,21},{2,26},{3,31},{4,20},{5,17},{6,30},{7,27},{8,24},{9,... | collective-permute-start | bytes 491528 | tf_op jit(solution)/shard_map/ppermute | solution.py:253
  11.0 16.7 %collective-permute-start = (bf16[128,128]{1,0:T(8,128)(2,1)S(1)}, bf16[128,128]{1,0:T(8,128)(2,1)S(1)}, u32[]{:S(2)}, u32[]{:S(2)}) collective-permute-start(bf16[128,128]{1,0:T(8,128)(2,1)S(1)} %get-tuple-element.15.kv_ref), channel_id=1, source_target_pairs={{0,4},{4,8},{8,12},{12,16},{16,20},{20,24},{24,28},{1,5},{5,9},{9,... | collective-permute-start | bytes 98312 | tf_op jit(solution)/shard_map/ppermute | solution.py:256
  14.4 9.8 %collective-permute-start.6 = (bf16[40,2048]{1,0:T(8,128)(2,1)S(1)}, bf16[40,2048]{1,0:T(8,128)(2,1)S(1)}, u32[]{:S(2)}, u32[]{:S(2)}) collective-permute-start(bf16[40,2048]{1,0:T(8,128)(2,1)S(1)} %collective-permute-done.4.refs_0_), channel_id=1, source_target_pairs={{0,2},{1,3},{2,0},{3,1},{4,6},{5,7},{6,4},{7,5},{8,10},{9,11},{10,... | collective-permute-start | bytes 491528 | tf_op jit(solution)/shard_map/ppermute | solution.py:286
  18.6 8.2 %collective-permute-start.10 = (bf16[40,2048]{1,0:T(8,128)(2,1)S(1)}, bf16[40,2048]{1,0:T(8,128)(2,1)S(1)}, u32[]{:S(2)}, u32[]{:S(2)}) collective-permute-start(bf16[40,2048]{1,0:T(8,128)(2,1)S(1)} %collective-permute-done.8.refs_4_), channel_id=1, source_target_pairs={{0,2},{1,3},{2,0},{3,1},{4,6},{5,7},{6,4},{7,5},{8,10},{9,11},{10,... | collective-permute-start | bytes 491528 | tf_op jit(solution)/shard_map/ppermute | solution.py:286
  23.6 19.3 %collective-permute-start.5 = (bf16[40,2048]{1,0:T(8,128)(2,1)S(1)}, bf16[40,2048]{1,0:T(8,128)(2,1)S(1)}, u32[]{:S(2)}, u32[]{:S(2)}) collective-permute-start(bf16[40,2048]{1,0:T(8,128)(2,1)S(1)} %collective-permute-done.4.refs_0_), channel_id=1, source_target_pairs={{0,1},{1,0},{2,3},{3,2},{4,5},{5,4},{6,7},{7,6},{8,9},{9,8},{10,11... | collective-permute-start | bytes 491528 | tf_op jit(solution)/shard_map/ppermute | solution.py:286
  23.6 19.2 %collective-permute-start.9 = (bf16[40,2048]{1,0:T(8,128)(2,1)S(1)}, bf16[40,2048]{1,0:T(8,128)(2,1)S(1)}, u32[]{:S(2)}, u32[]{:S(2)}) collective-permute-start(bf16[40,2048]{1,0:T(8,128)(2,1)S(1)} %collective-permute-done.8.refs_4_), channel_id=1, source_target_pairs={{0,1},{1,0},{2,3},{3,2},{4,5},{5,4},{6,7},{7,6},{8,9},{9,8},{10,11... | collective-permute-start | bytes 491528 | tf_op jit(solution)/shard_map/ppermute | solution.py:286
  24.1 18.7 %collective-permute-start.7 = (bf16[40,2048]{1,0:T(8,128)(2,1)S(1)}, bf16[40,2048]{1,0:T(8,128)(2,1)S(1)}, u32[]{:S(2)}, u32[]{:S(2)}) collective-permute-start(bf16[40,2048]{1,0:T(8,128)(2,1)S(1)} %collective-permute-done.6.refs_2_), channel_id=1, source_target_pairs={{0,1},{1,0},{2,3},{3,2},{4,5},{5,4},{6,7},{7,6},{8,9},{9,8},{10,11... | collective-permute-start | bytes 491528 | tf_op jit(solution)/shard_map/ppermute | solution.py:286
  26.8 16.0 %collective-permute-start.11 = (bf16[40,2048]{1,0:T(8,128)(2,1)S(1)}, bf16[40,2048]{1,0:T(8,128)(2,1)S(1)}, u32[]{:S(2)}, u32[]{:S(2)}) collective-permute-start(bf16[40,2048]{1,0:T(8,128)(2,1)S(1)} %collective-permute-done.10.refs_6_), channel_id=1, source_target_pairs={{0,1},{1,0},{2,3},{3,2},{4,5},{5,4},{6,7},{7,6},{8,9},{9,8},{10,11... | collective-permute-start | bytes 491528 | tf_op jit(solution)/shard_map/ppermute | solution.py:286
  27.6 6.1 %collective-permute-start.1 = (bf16[128,128]{1,0:T(8,128)(2,1)S(1)}, bf16[128,128]{1,0:T(8,128)(2,1)S(1)}, u32[]{:S(2)}, u32[]{:S(2)}) collective-permute-start(bf16[128,128]{1,0:T(8,128)(2,1)S(1)} %get-tuple-element.15.kv_ref), channel_id=1, source_target_pairs={{4,0},{8,4},{12,8},{16,12},{20,16},{24,20},{28,24},{5,1},{9,5},{13... | collective-permute-start | bytes 98312 | tf_op jit(solution)/shard_map/ppermute | solution.py:257
  33.7 1.2 %copy-start = (bf16[256,2048]{1,0:T(8,128)(2,1)S(1)}, bf16[256,2048]{1,0:T(8,128)(2,1)}, u32[]{:S(2)}) copy-start(bf16[256,2048]{1,0:T(8,128)(2,1)} %wo_ref.1) | copy-start | bytes 3145732
  35.0 0.8 %copy-start.2 = (bf16[128,256]{1,0:T(8,128)(2,1)S(1)}, bf16[128,256]{1,0:T(8,128)(2,1)}, u32[]{:S(2)}) copy-start(bf16[128,256]{1,0:T(8,128)(2,1)} %q_ref.1) | copy-start | bytes 196612
  35.8 0.7 copy-start.6
  48.6 2.2 %collective-permute-start.12 = (bf16[320,1024]{1,0:T(8,128)(2,1)S(1)}, bf16[320,1024]{1,0:T(8,128)(2,1)S(1)}, u32[]{:S(2)}, u32[]{:S(2)}) collective-permute-start(bf16[320,1024]{1,0:T(8,128)(2,1)S(1)} %get-tuple-element.25), channel_id=1, source_target_pairs={{0,1},{1,0},{2,3},{3,2},{4,5},{5,4},{6,7},{7,6},{8,9},{9,8},{10,11... | collective-permute-start | bytes 1966088 | tf_op jit(solution)/shard_map/ppermute | solution.py:303
  48.7 4.1 %collective-permute-start.2 = (bf16[64,2048]{1,0:T(8,128)(2,1)S(1)}, bf16[64,2048]{1,0:T(8,128)(2,1)S(1)}, u32[]{:S(2)}, u32[]{:S(2)}) collective-permute-start(bf16[64,2048]{1,0:T(8,128)(2,1)S(1)} %get-tuple-element.17), channel_id=1, source_target_pairs={{0,1},{1,0},{2,3},{3,2},{4,5},{5,4},{6,7},{7,6},{8,9},{9,8},{10,11... | collective-permute-start | bytes 786440 | tf_op jit(solution)/shard_map/ppermute | solution.py:304
  51.0 10.6 %collective-permute-start.13 = (bf16[320,512]{1,0:T(8,128)(2,1)S(1)}, bf16[320,512]{1,0:T(8,128)(2,1)S(1)}, u32[]{:S(2)}, u32[]{:S(2)}) collective-permute-start(bf16[320,512]{1,0:T(8,128)(2,1)S(1)} %get-tuple-element.27), channel_id=1, source_target_pairs={{0,2},{1,3},{2,0},{3,1},{4,6},{5,7},{6,4},{7,5},{8,10},{9,11},{10,... | collective-permute-start | bytes 983048 | tf_op jit(solution)/shard_map/ppermute | solution.py:303
  52.9 16.1 %collective-permute-start.3 = (bf16[32,2048]{1,0:T(8,128)(2,1)S(1)}, bf16[32,2048]{1,0:T(8,128)(2,1)S(1)}, u32[]{:S(2)}, u32[]{:S(2)}) collective-permute-start(bf16[32,2048]{1,0:T(8,128)(2,1)S(1)} %slice.9), channel_id=1, source_target_pairs={{0,2},{1,3},{2,0},{3,1},{4,6},{5,7},{6,4},{7,5},{8,10},{9,11},{10,... | collective-permute-start | bytes 393224 | tf_op jit(solution)/shard_map/ppermute | solution.py:304
  63.0 14.9 %all-to-all-start = ((bf16[8,40,512]{2,1,0:T(8,128)(2,1)}), bf16[8,40,512]{2,1,0:T(8,128)(2,1)S(1)}, u32[]{:S(2)}, u32[]{:S(2)}) async-start(bf16[8,40,512]{2,1,0:T(8,128)(2,1)} %last.1), calls=%async_computation | async-start | bytes 655360 | tf_op jit(solution)/shard_map/all_to_all | solution.py:328
